TPU v7x, 32 devices: a whole 2x2x4 slice. The times are simulated.
32 devices in a mesh: sp: 4 (over z), fs: 4 (over y, x), tp: 2 (over core).
Axes of the slice: x: 2, y: 2, z: 4, core: 2. Of those that a mesh axis runs over, the one named last changes fastest.
Arguments:
- tokens: bfloat16 [4, 4096, 2048], P('fs', ('sp', 'tp')), may hold values from -6 to 6
- norm_gain: bfloat16 [2048], replicated, may hold values from 0.099609375 to 1.8984375
- w_query: bfloat16 [2048, 1024], P(None, 'tp'), may hold values from -0.125 to 0.125
- w_key: bfloat16 [2048, 1024], P(None, 'tp'), may hold values from -0.125 to 0.125
- w_value: bfloat16 [2048, 1024], P(None, 'tp'), may hold values from -0.125 to 0.125
- w_outgate: bfloat16 [2048, 1024], P(None, 'tp'), may hold values from -0.125 to 0.125
- w_gatein: bfloat16 [2048, 1024], P(None, 'tp'), may hold values from -0.125 to 0.125
- w_gateout: bfloat16 [2048, 1024], P(None, 'tp'), may hold values from -0.125 to 0.125
- w_convin: bfloat16 [2048, 1024], P(None, 'tp'), may hold values from -0.125 to 0.125
- w_igate: bfloat16 [2048, 8], replicated, may hold values from -0.125 to 0.125
- w_fgate: bfloat16 [2048, 8], replicated, may hold values from -0.125 to 0.125
- input_bias: float32 [8], replicated, may hold values from -1 to 101
- forget_bias: float32 [8], replicated
- forget_extra: float32 [4, 4096, 8], P('fs', 'sp', 'tp'), may hold values from -0.7 to 0
- init_memory: float32 [4, 8, 128, 128], P('fs', 'tp'), may hold values from -56 to 56
- head_gain: bfloat16 [1024], replicated, may hold values from 0.099609375 to 1.8984375
- conv_taps: bfloat16 [3, 1024], replicated, may hold values from -3.5 to 3.5
- out_memory: bfloat16 [1024, 2048], P('tp'), may hold values from -0.125 to 0.125
- out_conv: bfloat16 [1024, 2048], P('tp'), may hold values from -0.125 to 0.125
Outputs:
- layer_out: bfloat16 [4, 4096, 2048], P('fs', ('sp', 'tp'))
All inputs are finite; a program needn't handle non-finite values.
Results may differ from a plain program's by a relative error of at most 0.017.
Values may be sent and summed in bfloat16 or wider, within the bound.
A program may use at most 128 MiB of HBM per device.

v0:
```python
import jax
import jax.numpy as jnp
from jax import lax
from jax.sharding import PartitionSpec as P

BLOCK = 128


EPSILON = 1e-06
LOWEST_LOG = -1e30


def shifted(block, axis, distance):
    devices = range(lax.axis_size(axis))
    route = [(i - distance, i) for i in devices if i - distance in devices]
    return lax.ppermute(block, axis, route)


def entering(part, axis, combine, identity):
    place = lax.axis_index(axis)
    gathered = jax.tree.map(lambda a: lax.all_gather(a, axis), part)
    state = jax.tree.map(lambda a, e: jnp.zeros_like(a) + jnp.asarray(e, a.dtype), part, identity)

    def one(step, state):
        return combine(
            state, jax.tree.map(lambda a: lax.dynamic_index_in_dim(a, step, 0, False), gathered)
        )

    return lax.fori_loop(0, place, one, state)


def compose(memory_pair, segment):
    memory, log_scale = memory_pair
    span_total, seg_memory, seg_scale = segment
    merged = jnp.maximum(span_total + log_scale, seg_scale)
    kept_share = jnp.exp(span_total + log_scale - merged)
    added_share = jnp.exp(seg_scale - merged)
    return (
        kept_share[..., None, None] * memory + added_share[..., None, None] * seg_memory,
        merged,
    )


def combine(earlier, later_part):
    memory, log_scale = compose((earlier[1], earlier[2]), later_part)
    return (earlier[0] + later_part[0], memory, log_scale)


def local(
    tokens,
    norm_gain,
    w_query,
    w_key,
    w_value,
    w_outgate,
    w_gatein,
    w_gateout,
    w_convin,
    w_igate,
    w_fgate,
    input_bias,
    forget_bias,
    forget_extra,
    init_memory,
    head_gain,
    conv_taps,
    out_memory,
    out_conv,
):
    local_heads = init_memory.shape[1]
    head_dim = init_memory.shape[-1]
    width_local = w_query.shape[1]
    key_factor = head_dim ** (-0.5)
    part_index = lax.axis_index("tp")
    own_rows = tokens[0].astype(jnp.float32)
    normed = own_rows * lax.rsqrt(jnp.mean(own_rows * own_rows, axis=-1, keepdims=True) + EPSILON)
    normed = (normed * norm_gain.astype(jnp.float32)).astype(jnp.bfloat16)
    normed_all = lax.all_gather(normed, "tp", axis=0, tiled=True)

    def project(weight):
        return jnp.dot(normed_all, weight, preferred_element_type=jnp.float32).astype(jnp.bfloat16)

    queries = project(w_query)
    key_rows = project(w_key)
    value_rows = project(w_value)
    out_gate = project(w_outgate)
    gate_in = project(w_gatein)
    gate_out = project(w_gateout)
    conv_input = project(w_convin)
    conv_product = (gate_in.astype(jnp.float32) * conv_input.astype(jnp.float32)).astype(
        jnp.bfloat16
    )
    token_count = normed_all.shape[0]
    tap_count = conv_taps.shape[0]
    rim_rows = shifted(conv_product[token_count - tap_count + 1 :], "sp", 1)
    head_start = part_index * local_heads
    gate_weights = jnp.concatenate(
        [
            lax.dynamic_slice_in_dim(w_igate, head_start, local_heads, 1),
            lax.dynamic_slice_in_dim(w_fgate, head_start, local_heads, 1),
        ],
        axis=1,
    )
    gate_pre = jnp.dot(normed_all, gate_weights, preferred_element_type=jnp.float32)
    input_pre = gate_pre[:, :local_heads] + lax.dynamic_slice_in_dim(
        input_bias, head_start, local_heads
    )
    forget_pre = gate_pre[:, local_heads:] + lax.dynamic_slice_in_dim(
        forget_bias, head_start, local_heads
    )
    log_forget = jax.nn.log_sigmoid(forget_pre) + forget_extra[0]
    nblocks = token_count // BLOCK
    block_shape = (nblocks, BLOCK, local_heads, head_dim)
    query_blocks = queries.reshape(block_shape)
    key_blocks = key_rows.reshape(block_shape)
    value_blocks = value_rows.reshape(block_shape)
    gate_in_blocks = jnp.swapaxes(input_pre.reshape(nblocks, BLOCK, local_heads), 1, 2)
    forget_blocks = jnp.swapaxes(log_forget.reshape(nblocks, BLOCK, local_heads), 1, 2)
    cumulative = jnp.cumsum(forget_blocks, axis=-1)
    block_total = cumulative[..., -1]
    exponent = block_total[..., None] - cumulative + gate_in_blocks
    block_top = jnp.max(exponent, axis=-1)
    key_weights = jnp.swapaxes(jnp.exp(exponent - block_top[..., None]), 1, 2)[..., None]
    weighted_keys = (key_weights * key_blocks.astype(jnp.float32) * key_factor).astype(jnp.bfloat16)
    block_terms = jnp.einsum(
        "bshd,bshe->bhde", weighted_keys, value_blocks, preferred_element_type=jnp.float32
    )
    identity = (
        jnp.zeros((local_heads,), jnp.float32),
        jnp.zeros((local_heads, head_dim, head_dim), jnp.float32),
        jnp.full((local_heads,), LOWEST_LOG, jnp.float32),
    )

    def block_step(running, element):
        return (combine(running, element), running)

    segment, prefixes = lax.scan(block_step, identity, (block_total, block_terms, block_top))
    start_pair = (init_memory[0], jnp.zeros((local_heads,), jnp.float32))
    earlier = entering(segment, "sp", combine, identity)
    incoming = compose(start_pair, earlier)
    starts_memory, starts_scale = compose(incoming, prefixes)
    row_index = lax.broadcasted_iota(jnp.int32, (BLOCK, BLOCK), 0)
    col_index = lax.broadcasted_iota(jnp.int32, (BLOCK, BLOCK), 1)
    pair_log = cumulative[..., :, None] - cumulative[..., None, :] + gate_in_blocks[..., None, :]
    pair_log = jnp.where(col_index <= row_index, pair_log, -jnp.inf)
    carried_log = cumulative + starts_scale[..., None]
    row_top = jnp.maximum(carried_log, jnp.max(pair_log, axis=-1))
    scores = (
        jnp.einsum("bthd,bshd->bhts", query_blocks, key_blocks, preferred_element_type=jnp.float32)
        * key_factor
    )
    weighted = (jnp.exp(pair_log - row_top[..., None]) * scores).astype(jnp.bfloat16)
    carried = jnp.einsum(
        "bthd,bhde->bthe",
        query_blocks.astype(jnp.float32),
        starts_memory,
        precision=lax.Precision.HIGHEST,
    )
    inter_weight = jnp.swapaxes(jnp.exp(carried_log - row_top), 1, 2)[..., None]
    readout = inter_weight * carried + jnp.einsum(
        "bhts,bshe->bthe", weighted, value_blocks, preferred_element_type=jnp.float32
    )
    normalized = readout * lax.rsqrt(jnp.mean(readout * readout, axis=-1, keepdims=True) + EPSILON)
    gain_local = lax.dynamic_slice_in_dim(head_gain, part_index * width_local, width_local).astype(
        jnp.float32
    )
    memory_out = (
        normalized.reshape(token_count, width_local)
        * gain_local
        * jax.nn.sigmoid(out_gate.astype(jnp.float32))
    )
    memory_out = memory_out.astype(jnp.bfloat16)
    taps_local = lax.dynamic_slice_in_dim(
        conv_taps, part_index * width_local, width_local, 1
    ).astype(jnp.float32)
    padded = jnp.concatenate([rim_rows, conv_product], axis=0).astype(jnp.float32)
    mixed_conv = padded[0:token_count] * taps_local[0]
    for tap_index in range(1, tap_count):
        mixed_conv = (
            mixed_conv + padded[tap_index : tap_index + token_count] * taps_local[tap_index]
        )
    conv_out = (gate_out.astype(jnp.float32) * mixed_conv).astype(jnp.bfloat16)
    layer_rows = lax.psum_scatter(
        (
            jnp.dot(memory_out, out_memory, preferred_element_type=jnp.float32)
            + jnp.dot(conv_out, out_conv, preferred_element_type=jnp.float32)
        ).astype(jnp.bfloat16),
        "tp",
        scatter_dimension=0,
        tiled=True,
    )
    return layer_rows[None]


def solution(mesh):
    return jax.shard_map(
        local,
        mesh=mesh,
        in_specs=(
            P("fs", ("sp", "tp"), None),
            P(),
            P(None, "tp"),
            P(None, "tp"),
            P(None, "tp"),
            P(None, "tp"),
            P(None, "tp"),
            P(None, "tp"),
            P(None, "tp"),
            P(),
            P(),
            P(),
            P(),
            P("fs", "sp", "tp"),
            P("fs", "tp", None, None),
            P(),
            P(),
            P("tp", None),
            P("tp", None),
        ),
        out_specs=P("fs", ("sp", "tp"), None),
        check_vma=False,
    )
```

profile of v0, /device:TPU:0, one launch (start us, length us, event | category | flops | bytes accessed | tf_op | source)
XLA Modules:
  0.0 161.9 jit_solution(6169005521759657733)
XLA Ops:
  6.5 2.2 %fusion.14 = f32[512]{0:T(512)S(1)} fusion(bf16[1,512,2048]{2,1,0:T(8,128)(2,1)} %param.23), kind=kLoop, calls=%fused_computation.30 | loop fusion | flops 3145216 | bytes 2099200 | tf_op jit(solution)/shard_map/reduce_sum | solution.py:76
  8.9 1.9 %fusion.16 = bf16[512,2048]{1,0:T(8,128)(2,1)} fusion(bf16[1,512,2048]{2,1,0:T(8,128)(2,1)S(1)} %copy-done.2, f32[2048]{0:T(1024)S(1)} %convert_element_type.78, f32[512]{0:T(512)S(1)} %add_rsqrt_fusion.1), kind=kLoop, calls=%fused_computation.32 | loop fusion | flops 4194304 | bytes 4204544 | tf_op jit(solution)/shard_map/convert_element_type | solution.py:77
  13.0 14.4 %all-gather.6.cloned.1.call-done = bf16[1024,2048]{1,0:T(8,128)(2,1)} async-done(((bf16[512,2048]{1,0:T(8,128)(2,1)}), bf16[1024,2048]{1,0:T(8,128)(2,1)}) %all-gather.6.cloned.1.call-update) | async-done | bytes 4194320 | tf_op jit(solution)/shard_map/all_gather | solution.py:78
  27.4 3.4 %fusion.49 = f32[1024,8]{0,1:T(8,128)S(1)} fusion(bf16[1024,2048]{1,0:T(8,128)(2,1)} %all-gather.6.cloned.1.call-done, bf16[2048,4]{0,1:T(4,128)(2,1)S(1)} %get-tuple-element.236, bf16[2048,4]{0,1:T(4,128)(2,1)S(1)} %get-tuple-element.237), kind=kOutput, calls=%fused_computation.85 | convolution fusion | flops 33619968 | bytes 4259840 | tf_op jit(solution)/shard_map/dot_general | solution.py:104
  32.7 6.2 %convolution_convert_fusion.5 = bf16[1024,512]{1,0:T(8,128)(2,1)} fusion(bf16[1024,2048]{1,0:T(8,128)(2,1)} %all-gather.6.cloned.1.call-done, bf16[2048,512]{1,0:T(8,128)(2,1)} %param.27), kind=kOutput, calls=%fused_computation.61 | convolution fusion | flops 2148007936 | bytes 7340032 | tf_op jit(solution)/shard_map/dot_general | solution.py:81
  40.2 1.3 copy.66
  41.5 6.2 %convolution_convert_fusion.6 = bf16[1024,512]{1,0:T(8,128)(2,1)} fusion(bf16[1024,2048]{1,0:T(8,128)(2,1)} %all-gather.6.cloned.1.call-done, bf16[2048,512]{1,0:T(8,128)(2,1)} %param.26), kind=kOutput, calls=%fused_computation.62 | convolution fusion | flops 2148007936 | bytes 7340032 | tf_op jit(solution)/shard_map/dot_general | solution.py:81
  49.0 1.3 copy.50
  50.4 3.7 %fusion.31 = f32[8,4,128,128]{3,2,1,0:T(8,128)} fusion(bf16[8,128,4,128]{1,3,2,0:T(8,128)(2,1)} %copy.66, bf16[8,128,4,128]{1,3,2,0:T(8,128)(2,1)} %copy.50, f32[8,128,4]{1,2,0:T(4,128)S(1)} %copy.49), kind=kOutput, calls=%fused_computation.64 | convolution fusion | flops 136314880 | bytes 4210688 | tf_op jit(solution)/shard_map/bshd,bshe->bhde/dot_general | solution.py:125
  54.1 15.3 %while.36 = (s32[]{:T(128)}, f32[4]{0:T(128)S(1)}, f32[4,128,128]{2,1,0:T(8,128)S(1)}, f32[4]{0:T(128)S(1)}, f32[8,4]{1,0:T(8,128)S(1)}, /*index=5*/f32[8,4,128,...) while((s32[]{:T(128)}, f32[4]{0:T(128)S(1)}, ...), condition=%wide.region_4.5_spmd.clone, body=%wide.region_3.4_spmd.clone.sunk | while | flops 327711 | bytes 1311169 | solution.py:137
  70.2 5.3 %convolution_convert_fusion = bf16[1024,512]{1,0:T(8,128)(2,1)S(1)} fusion(bf16[1024,2048]{1,0:T(8,128)(2,1)} %all-gather.6.cloned.1.call-done, bf16[2048,512]{1,0:T(8,128)(2,1)} %param.31), kind=kOutput, calls=%fused_computation.56 | convolution fusion | flops 2148007936 | bytes 7340032 | tf_op jit(solution)/shard_map/dot_general | solution.py:81
  75.6 2.3 %multiply_convert_fusion = bf16[1024,512]{1,0:T(8,128)(2,1)S(1)} fusion(bf16[1024,512]{1,0:T(8,128)(2,1)S(1)} %convolution_convert_fusion, bf16[1024,2048]{1,0:T(8,128)(2,1)S(1)} %copy-done.3, bf16[2048,512]{1,0:T(8,128)(2,1)S(1)} %copy-done.11), kind=kOutput, calls=%fused_computation.45 | convolution fusion | flops 2150105088 | bytes 8388608 | tf_op jit(solution)/shard_map/dot_general | solution.py:81
  77.9 3.8 %collective-permute-start = (bf16[2,512]{1,0:T(2,128)(2,1)S(1)}, bf16[2,512]{1,0:T(2,128)(2,1)S(1)}, u32[]{:S(2)}, u32[]{:S(2)}) collective-permute-start(bf16[2,512]{1,0:T(2,128)(2,1)S(1)} %slice.43), channel_id=1, source_target_pairs={{0,8},{8,16},{16,24},{1,9},{9,17},{17,25},{2,10},{10,18},{18,26},{... | collective-permute-start | bytes 6152 | tf_op jit(solution)/shard_map/ppermute | solution.py:16
  81.8 3.3 %convolution_convert_fusion.4 = bf16[1024,512]{1,0:T(8,128)(2,1)} fusion(bf16[1024,2048]{1,0:T(8,128)(2,1)S(1)} %copy-done.3, bf16[2048,512]{1,0:T(8,128)(2,1)S(1)} %copy-done.12), kind=kOutput, calls=%fused_computation.60 | convolution fusion | flops 2148007936 | bytes 7340032 | tf_op jit(solution)/shard_map/dot_general | solution.py:81
  86.4 2.2 %reshape.67 = bf16[8,128,4,128]{3,2,1,0:T(4,128)(2,1)} reshape(bf16[1024,512]{1,0:T(8,128)(2,1)} %convolution_convert_fusion.4) | data formatting | bytes 2097152 | tf_op jit(solution)/shard_map/reshape | solution.py:114
  88.9 10.3 %all-reduce.2 = (f32[16]{0:T(128)S(1)}, f32[16]{0:T(128)S(1)}) all-reduce(f32[16]{0:T(128)S(1)} %dynamic-update-slice, f32[16]{0:T(128)S(1)} %dynamic-update-slice.1), channel_id=2, replica_groups=mesh['sp'=4,'fs'=4,'tp'=2] {'sp'}, use_global_device_ids=true, to_apply=%add | all-reduce | flops 32 | bytes 256
  99.4 1.7 %maximum_convert_fusion = f32[1026,512]{1,0:T(8,128)} fusion(bf16[1024,512]{1,0:T(8,128)(2,1)S(1)} %multiply_convert_fusion, bf16[2,512]{1,0:T(2,128)(2,1)S(1)} %collective-permute-done), kind=kLoop, calls=%fused_computation.63 | loop fusion | flops 2101248 | bytes 3151872 | tf_op jit(solution)/shard_map/convert_element_type | solution.py:176
  102.3 3.9 %fusion.30 = f32[8,4,128,128]{3,2,1,0:T(8,128)} fusion(bf16[8,128,4,128]{1,3,2,0:T(8,128)(2,1)S(1)} %copy-done.4, bf16[8,128,4,128]{1,3,2,0:T(8,128)(2,1)} %copy.50, f32[8,4,128]{2,1,0:T(4,128)S(1)} %copy.63, f32[8,4,128]{2,1,0:T(4,128)S(1)} %copy.57, f32[8,4,128]{2,1,0:T(4,128)S(1)} %copy.55, pred[128,128]{1,0:T(8,128)(4,1)S(1)} %iota_compare_fusion, ...), kind=kOutput, calls=%fused_computation.55 | convolution fusion | flops 272105472 | bytes 5308416 | tf_op jit(solution)/shard_map/bhts,bshe->bthe/dot_general | solution.py:160
  107.3 4.7 %multiply_reduce_fusion = (f32[8,128,4]{1,2,0:T(4,128)S(1)}, f32[8,128,4,128]{1,3,2,0:T(8,128)S(1)}) fusion(f32[8,4,128,128]{3,2,1,0:T(8,128)} %fusion.30, bf16[8,128,4,128]{3,2,1,0:T(4,128)(2,1)} %reshape.67, f32[8,4,128,128]{3,2,1,0:T(8,128)} %get-tuple-element.115, f32[8,4]{1,0:T(8,128)S(1)} %subtract_exponential_fusion.4, ...), kind=kOutput, calls=%fused_computation.46 | convolution fusion | flops 808972288 | bytes 7635200 | tf_op jit(solution)/shard_map/bthd,bhde->bthe/dot_general | solution.py:153
  112.0 1.5 broadcast_multiply_fusion
  113.5 2.9 %copy.70 = f32[8,128,4,128]{3,2,1,0:T(4,128)} copy(f32[8,128,4,128]{1,3,2,0:T(8,128)} %broadcast_multiply_fusion) | data formatting | bytes 4194304 | tf_op jit(solution)/shard_map/reshape | solution.py:168
  116.4 11.3 %fusion.47 = f32[1024,2048]{1,0:T(8,128)} fusion(bf16[512,2048]{1,0:T(8,128)(2,1)S(1)} %copy-done, f32[128,8,4,128]{3,2,1,0:T(4,128)} %bitcast.151, bf16[1024,2048]{1,0:T(8,128)(2,1)} %all-gather.6.cloned.1.call-done, bf16[2048,512]{1,0:T(8,128)(2,1)} %param.28, f32[512]{0:T(512)S(1)} %dynamic-slice_convert_fusion.1), kind=kOutput, calls=%fused_computation.80 | convolution fusion | flops 4299161600 | bytes 18876416 | tf_op jit(solution)/shard_map/dot_general | solution.py:185
  127.7 14.4 %add_convert_fusion = bf16[1024,2048]{1,0:T(8,128)(2,1)} fusion(f32[1024,2048]{1,0:T(8,128)} %fusion.47, bf16[512,2048]{1,0:T(8,128)(2,1)} %param.41, f32[1026,512]{1,0:T(8,128)} %maximum_convert_fusion, bf16[1024,2048]{1,0:T(8,128)(2,1)} %all-gather.6.cloned.1.call-done, bf16[2048,512]{1,0:T(8,128)(2,1)} %param.30, f32[512]{0:T(512)S(1)} %bitcast.156, ...), kind=kOutput, calls=%fused_computation.27 | convolution fusion | flops 4303880192 | bytes 27269120 | tf_op jit(solution)/shard_map/dot_general | solution.py:186
  142.1 13.3 %reduce-scatter.2.cloned.1.call-done = bf16[512,2048]{1,0:T(8,128)(2,1)} async-done(((bf16[1024,2048]{1,0:T(8,128)(2,1)}), bf16[512,2048]{1,0:T(8,128)(2,1)}) %reduce-scatter.2.cloned.1.call-update) | async-done | bytes 2097168 | tf_op jit(solution)/shard_map/reduce_scatter | solution.py:183
  (141 shorter events, 26.1 us)
Async XLA Ops:
  6.5 109.8 %copy-start = (bf16[512,2048]{1,0:T(8,128)(2,1)S(1)}, bf16[512,2048]{1,0:T(8,128)(2,1)}, u32[]{:S(2)}) copy-start(bf16[512,2048]{1,0:T(8,128)(2,1)} %param.40) | copy-start | bytes 6291460
  6.5 2.2 %copy-start.8 = (bf16[2048]{0:T(1024)(128)(2,1)S(1)}, bf16[2048]{0:T(1024)(128)(2,1)}, u32[]{:S(2)}) copy-start(bf16[2048]{0:T(1024)(128)(2,1)} %param.24) | copy-start | bytes 12292
  6.5 20.9 %all-gather.6.cloned.1.call-start = ((), (), s32[]{:S(2)}) async-start(), calls=%async_computation.1 | async-start | bytes 6291456 | tf_op jit(solution)/shard_map/all_gather | solution.py:78
  6.5 2.4 %copy-start.2 = (bf16[1,512,2048]{2,1,0:T(8,128)(2,1)S(1)}, bf16[1,512,2048]{2,1,0:T(8,128)(2,1)}, u32[]{:S(2)}) copy-start(bf16[1,512,2048]{2,1,0:T(8,128)(2,1)} %param.23) | copy-start | bytes 6291460
  10.8 0.7 copy-start.13
  10.8 0.7 copy-start.14
  10.8 0.8 copy-start.15
  10.8 2.0 %copy-start.10 = (bf16[1024]{0:T(1024)(128)(2,1)S(1)}, bf16[1024]{0:T(1024)(128)(2,1)}, u32[]{:S(2)}) copy-start(bf16[1024]{0:T(1024)(128)(2,1)} %param.38) | copy-start | bytes 6148
  10.8 2.1 %copy-start.9 = (bf16[3,1024]{1,0:T(4,128)(2,1)S(1)}, bf16[3,1024]{1,0:T(4,128)(2,1)}, u32[]{:S(2)}) copy-start(bf16[3,1024]{1,0:T(4,128)(2,1)} %param.39) | copy-start | bytes 18436
  10.8 2.1 %copy-start.6 = (bf16[2048,8]{0,1:T(8,128)(2,1)S(1)}, bf16[2048,8]{0,1:T(8,128)(2,1)}, u32[]{:S(2)}) copy-start(bf16[2048,8]{0,1:T(8,128)(2,1)} %param.33) | copy-start | bytes 98308
  10.8 2.1 %copy-start.7 = (bf16[2048,8]{0,1:T(8,128)(2,1)S(1)}, bf16[2048,8]{0,1:T(8,128)(2,1)}, u32[]{:S(2)}) copy-start(bf16[2048,8]{0,1:T(8,128)(2,1)} %param.32) | copy-start | bytes 98308
  10.9 90.2 %all-gather.8.cloned.1.call-start = ((), (), s32[]{:S(2)}) async-start(), calls=%async_computation.3 | async-start | bytes 1310720 | tf_op jit(solution)/shard_map/all_gather | solution.py:21
  27.4 3.4 %copy-start.5 = (f32[1,1024,4]{1,2,0:T(4,128)S(1)}, f32[1,1024,4]{1,2,0:T(4,128)}, u32[]{:S(2)}) copy-start(f32[1,1024,4]{1,2,0:T(4,128)} %param.36) | copy-start | bytes 49156
  69.4 0.7 copy-start.1
  70.1 85.3 %reduce-scatter.2.cloned.1.call-start = ((), (), s32[]{:S(2)}) async-start(), calls=%async_computation.2 | async-start | bytes 6291456 | tf_op jit(solution)/shard_map/reduce_scatter | solution.py:183
  70.2 5.4 %copy-start.3 = (bf16[1024,2048]{1,0:T(8,128)(2,1)S(1)}, bf16[1024,2048]{1,0:T(8,128)(2,1)}, u32[]{:S(2)}) copy-start(bf16[1024,2048]{1,0:T(8,128)(2,1)} %all-gather.6.cloned.1.call-done) | copy-start | bytes 12582916
  70.2 5.4 %copy-start.11 = (bf16[2048,512]{1,0:T(8,128)(2,1)S(1)}, bf16[2048,512]{1,0:T(8,128)(2,1)}, u32[]{:S(2)}) copy-start(bf16[2048,512]{1,0:T(8,128)(2,1)} %param.29) | copy-start | bytes 6291460
  75.5 6.2 %copy-start.12 = (bf16[2048,512]{1,0:T(8,128)(2,1)S(1)}, bf16[2048,512]{1,0:T(8,128)(2,1)}, u32[]{:S(2)}) copy-start(bf16[2048,512]{1,0:T(8,128)(2,1)} %param.25) | copy-start | bytes 6291460
  77.9 21.5 %collective-permute-start = (bf16[2,512]{1,0:T(2,128)(2,1)S(1)}, bf16[2,512]{1,0:T(2,128)(2,1)S(1)}, u32[]{:S(2)}, u32[]{:S(2)}) collective-permute-start(bf16[2,512]{1,0:T(2,128)(2,1)S(1)} %slice.43), channel_id=1, source_target_pairs={{0,8},{8,16},{16,24},{1,9},{9,17},{17,25},{2,10},{10,18},{18,26},{... | collective-permute-start | bytes 6152 | tf_op jit(solution)/shard_map/ppermute | solution.py:16
  101.1 1.2 copy-start.4
Sparse Core Ops, SparseCore 0:
  11.0 16.3 all-gather.5
  70.2 29.4 all-gather.7
  142.2 13.0 reduce-scatter.1
where the time goes:
time: 163 us; the launch traced here: 162 us
  matrix products  64.6 us (40%)
  waiting for transfers between devices  27.7 us (17%)
  other arithmetic  25.9 us (16%)
  local copies, waits for them, and re-layouts  15 us (9%)
  between operations  14.1 us (9%)
  blocking collectives  10.3 us (6%)
  starting transfers between devices  3.92 us (2%)
    dot_general x5, matrix products, project(): jnp.dot(normed_all, weight, preferred_element_type=jnp.float32)  23.3 us
    all_gather x1, waiting for transfers between devices, local(): normed_all = lax.all_gather(normed, 'tp', axis=0, tiled=True)  14.4 us
    dot_general x1, matrix products, local(): jnp.dot(conv_out, out_conv, preferred_element_type=jnp.float32)  14.4 us
    reduce_scatter x1, waiting for transfers between devices, local(): lax.psum_scatter((jnp.dot(memory_out, out_memory, preferred_element_type=...  13.3 us
    dot_general x1, matrix products, local(): jnp.dot(memory_out, out_memory, preferred_element_type=jnp.float32)  11.3 us
    unnamed x1, blocking collectives  10.3 us
    add x9, other arithmetic, compose(): kept_share[..., None, None] * memory  9.44 us
    dynamic_update_slice x8, other arithmetic, local(): lax.scan(block_step, identity, (block_total, block_terms, block_top))  5.83 us
  transfers between devices with their start and end apart: 4, of which 2 were waited for; matrix products, arithmetic and copies ran while one was open for 11% of the time, Pallas kernels for 0%

commit v1 on v0

v1 whole, which is shorter than its diff:
```python
import functools

import jax
import jax.numpy as jnp
from jax import lax
from jax.experimental import pallas as pl
from jax.experimental.pallas import tpu as pltpu
from jax.sharding import PartitionSpec as P

BLOCK = 128
EPSILON = 1e-06
LOWEST_LOG = -1e30
MESH = pl.DeviceIdType.MESH
F32 = jnp.float32
BF16 = jnp.bfloat16
PAD = 8
RIM = 16
NORM_ROWS = 64
OUT_COLS = 512

KEY, VALUE, GATE_IN, CONV_IN, GATE_OUT, QUERY, OUT_GATE = range(7)


def kernel(
    n_sp,
    tokens,
    norm_gain,
    w_key,
    w_value,
    w_gatein,
    w_convin,
    w_gateout,
    w_query,
    w_outgate,
    gate_w,
    gate_bias,
    extra,
    init_memory,
    head_gain,
    conv_taps,
    out_memory,
    out_conv,
    layer_out,
    tok,
    normed,
    weights,
    out_w,
    proj,
    gate_pre,
    row_log,
    col_log,
    block_sum,
    block_peak,
    terms,
    running,
    running_log,
    starts,
    starts_log,
    seg_memory,
    seg_log,
    got_memory,
    got_log,
    conv_rows,
    rim,
    mix,
    part_send,
    part_got,
    result,
    local_sem,
    weight_sem,
    out_sem,
    token_sem,
    seg_send,
    seg_recv,
    rim_sem,
    part_sem_send,
    part_sem_recv,
):
    me = lax.axis_index("tp")
    other = 1 - me
    place = lax.axis_index("sp")
    half = tok.shape[1]
    total_rows = normed.shape[0]
    width = w_key.shape[1]
    heads = init_memory.shape[0]
    dh = init_memory.shape[1]
    nblocks = total_rows // BLOCK
    key_factor = dh ** (-0.5)
    out_width = layer_out.shape[1]
    n_out = out_width // OUT_COLS

    barrier = pltpu.get_barrier_semaphore()
    pl.semaphore_signal(barrier, inc=1, device_id={"tp": other}, device_id_type=MESH)
    for d in range(1, n_sp):
        pl.semaphore_signal(
            barrier, inc=1, device_id={"sp": lax.rem(place + d, n_sp)}, device_id_type=MESH
        )

    own_copy = pltpu.make_async_copy(tokens, tok.at[0], local_sem.at[0])
    own_copy.start()
    w_in = (w_key, w_value, w_gatein, w_convin, w_gateout, w_query, w_outgate)
    w_copies = [
        pltpu.make_async_copy(w, weights.at[s], weight_sem.at[s]) for s, w in enumerate(w_in)
    ]
    out_copies = [
        pltpu.make_async_copy(out_memory, out_w.at[pl.ds(0, width)], weight_sem.at[7]),
        pltpu.make_async_copy(out_conv, out_w.at[pl.ds(width, width)], weight_sem.at[8]),
    ]
    for c in w_copies + out_copies:
        c.start()

    pl.semaphore_wait(barrier, n_sp)
    token_copy = pltpu.make_async_remote_copy(
        src_ref=tokens,
        dst_ref=tok.at[1],
        send_sem=token_sem.at[0],
        recv_sem=token_sem.at[1],
        device_id={"tp": other},
        device_id_type=MESH,
    )
    token_copy.start()
    own_copy.wait()

    def rows_of(index, size):
        return pl.ds(pl.multiple_of(index * size, size), size)

    def normalize(slot, base):
        @pl.loop(0, half // NORM_ROWS)
        def _(c):
            x = tok[slot, rows_of(c, NORM_ROWS), :].astype(F32)
            scale = lax.rsqrt(jnp.mean(x * x, axis=-1, keepdims=True) + EPSILON)
            y = (x * scale) * norm_gain[...].astype(F32)
            normed[pl.ds(pl.multiple_of(base + c * NORM_ROWS, NORM_ROWS), NORM_ROWS), :] = y.astype(
                BF16
            )

    def project(slot, rows):
        proj[slot, rows, :] = jnp.dot(
            normed[rows, :], weights[slot], preferred_element_type=F32
        ).astype(BF16)

    @pl.loop(0, 2)
    def _(step):
        index = lax.rem(me + step, 2)

        @pl.when(step == 1)
        def _():
            token_copy.wait_recv()

        normalize(step, index * half)
        rows = rows_of(index, half)
        gate_pre[rows, :] = jnp.dot(normed[rows, :], gate_w[...], preferred_element_type=F32)

        @pl.loop(KEY, VALUE + 1)
        def _(slot):
            @pl.when(step == 0)
            def _():
                pltpu.make_async_copy(w_key, weights.at[slot], weight_sem.at[slot]).wait()

            project(slot, rows)

    row_i = lax.broadcasted_iota(jnp.int32, (BLOCK, BLOCK), 0)
    col_i = lax.broadcasted_iota(jnp.int32, (BLOCK, BLOCK), 1)
    upper = jnp.where(row_i <= col_i, 1.0, 0.0).astype(F32)
    for h in range(heads):
        running[h] = jnp.zeros((dh, dh), F32)
    running_log[0:PAD] = jnp.full((PAD, BLOCK), LOWEST_LOG, F32)
    running_log[PAD : 2 * PAD] = jnp.zeros((PAD, BLOCK), F32)

    def head_cols(h):
        return slice(h * dh, (h + 1) * dh)

    @pl.loop(0, nblocks)
    def _(b):
        rows = rows_of(b, BLOCK)
        pre = jnp.transpose(gate_pre[rows, :])
        v = pre[0:PAD] + gate_bias[0:PAD]
        log_forget = jnp.minimum(v, 0.0) - jnp.log1p(jnp.exp(-jnp.abs(v))) + extra[:, rows]
        gate_in = pre[PAD : 2 * PAD] + gate_bias[PAD : 2 * PAD]
        cumulative = jnp.dot(
            log_forget, upper, precision=lax.Precision.HIGHEST, preferred_element_type=F32
        )
        total = cumulative[:, BLOCK - 1 : BLOCK]
        exponent = total - cumulative + gate_in
        peak = jnp.max(exponent, axis=1, keepdims=True)
        key_weight = jnp.exp(exponent - peak)
        row_log[b, 0:PAD] = cumulative
        row_log[b, PAD : 2 * PAD] = gate_in
        stacked = jnp.concatenate(
            [cumulative, key_weight, jnp.zeros((BLOCK - 2 * PAD, BLOCK), F32)], axis=0
        )
        columns = jnp.transpose(stacked)
        col_log[b] = columns
        total = jnp.broadcast_to(total, (PAD, BLOCK))
        peak = jnp.broadcast_to(peak, (PAD, BLOCK))
        block_sum[b] = total
        block_peak[b] = peak
        old_log = running_log[0:PAD]
        merged = jnp.maximum(total + old_log, peak)
        keep = jnp.exp(total + old_log - merged)
        add = jnp.exp(peak - merged)
        running_log[0:PAD] = merged
        running_log[PAD : 2 * PAD] = running_log[PAD : 2 * PAD] + total
        for h in range(heads):
            k = proj[KEY, rows, head_cols(h)].astype(F32)
            wk = (columns[:, PAD + h : PAD + h + 1] * k * key_factor).astype(BF16)
            term = lax.dot_general(
                wk,
                proj[VALUE, rows, head_cols(h)],
                (((0,), (0,)), ((), ())),
                preferred_element_type=F32,
            )
            terms[b, h] = term
            running[h] = keep[h : h + 1] * running[h] + add[h : h + 1] * term

    for h in range(heads):
        seg_memory[h] = running[h].astype(BF16)
    seg_log[...] = running_log[...]

    def seg_copies(target, source, d):
        return [
            pltpu.make_async_remote_copy(
                src_ref=src,
                dst_ref=dst.at[source],
                send_sem=seg_send.at[which, d],
                recv_sem=seg_recv.at[which, source],
                device_id={"sp": target},
                device_id_type=MESH,
            )
            for which, (src, dst) in enumerate(((seg_memory, got_memory), (seg_log, got_log)))
        ]

    for d in range(1, n_sp):

        @pl.when(place + d < n_sp)
        def _(d=d):
            for c in seg_copies(place + d, place, d - 1):
                c.start()

    def finish(slots):
        @pl.loop(slots[0], slots[1])
        def _(slot):
            pltpu.make_async_copy(w_key, weights.at[slot], weight_sem.at[slot]).wait()

            @pl.loop(0, 2)
            def _(index):
                project(slot, rows_of(index, half))

    finish((GATE_IN, CONV_IN + 1))

    @pl.loop(0, nblocks)
    def _(b):
        rows = rows_of(b, BLOCK)
        product = proj[GATE_IN, rows, :].astype(F32) * proj[CONV_IN, rows, :].astype(F32)
        conv_rows[pl.ds(pl.multiple_of(RIM + b * BLOCK, RIM), BLOCK), :] = product.astype(BF16)

    next_place = lax.rem(place + 1, n_sp)
    rim_copy = pltpu.make_async_remote_copy(
        src_ref=conv_rows.at[pl.ds(total_rows, RIM)],
        dst_ref=rim,
        send_sem=rim_sem.at[0],
        recv_sem=rim_sem.at[1],
        device_id={"sp": next_place},
        device_id_type=MESH,
    )

    @pl.when(place + 1 < n_sp)
    def _():
        rim_copy.start()

    finish((GATE_OUT, OUT_GATE + 1))

    @pl.when(place > 0)
    def _():
        rim_copy.wait_recv()
        conv_rows[0:RIM, :] = rim[...]

    @pl.when(place == 0)
    def _():
        conv_rows[0:RIM, :] = jnp.zeros((RIM, width), BF16)

    own_cols = pl.ds(pl.multiple_of(me * width, width), width)
    taps = conv_taps[:, own_cols].astype(F32)
    tap_count = conv_taps.shape[0]

    @pl.loop(0, nblocks)
    def _(b):
        rows = rows_of(b, BLOCK)
        x = conv_rows[pl.ds(pl.multiple_of(b * BLOCK, RIM), BLOCK + RIM), :].astype(F32)
        mixed = None
        for j in range(tap_count):
            back = tap_count - 1 - j
            y = x if back == 0 else pltpu.roll(x, back, 0)
            y = y[RIM:] * taps[j : j + 1]
            mixed = y if mixed is None else mixed + y
        mix[rows, pl.ds(width, width)] = (proj[GATE_OUT, rows, :].astype(F32) * mixed).astype(BF16)

    for h in range(heads):
        running[h] = init_memory[h]
    running_log[0:PAD] = jnp.zeros((PAD, BLOCK), F32)

    def advance(total, peak, term_of):
        old_log = running_log[0:PAD]
        merged = jnp.maximum(total + old_log, peak)
        keep = jnp.exp(total + old_log - merged)
        add = jnp.exp(peak - merged)
        running_log[0:PAD] = merged
        for h in range(heads):
            running[h] = keep[h : h + 1] * running[h] + add[h : h + 1] * term_of(h)

    @pl.loop(0, place)
    def _(source):
        for c in seg_copies(place, source, 0):
            c.wait_recv()
        advance(
            got_log[source, PAD : 2 * PAD],
            got_log[source, 0:PAD],
            lambda h: got_memory[source, h].astype(F32),
        )

    @pl.loop(0, nblocks)
    def _(b):
        starts_log[b] = running_log[0:PAD]
        for h in range(heads):
            starts[b, h] = running[h].astype(BF16)
        advance(block_sum[b], block_peak[b], lambda h: terms[b, h])

    gain = head_gain[:, own_cols].astype(F32)
    causal = col_i <= row_i

    def readout(index):
        @pl.loop(0, half // BLOCK)
        def _(step):
            b = index * (half // BLOCK) + step
            rows = rows_of(b, BLOCK)
            columns = col_log[b]
            for h in range(heads):
                q = proj[QUERY, rows, head_cols(h)]
                k = proj[KEY, rows, head_cols(h)]
                scores = lax.dot_general(
                    q, k, (((1,), (1,)), ((), ())), preferred_element_type=F32
                )
                cum_col = columns[:, h : h + 1]
                pair = (cum_col - row_log[b, h : h + 1]) + row_log[b, PAD + h : PAD + h + 1]
                pair = jnp.where(causal, pair, -jnp.inf)
                carried_log = cum_col + starts_log[b, h : h + 1, 0:1]
                top = jnp.maximum(carried_log, jnp.max(pair, axis=1, keepdims=True))
                weighted = (jnp.exp(pair - top) * (scores * key_factor)).astype(BF16)
                carried = jnp.dot(q, starts[b, h], preferred_element_type=F32)
                out = jnp.exp(carried_log - top) * carried + jnp.dot(
                    weighted, proj[VALUE, rows, head_cols(h)], preferred_element_type=F32
                )
                out = out * lax.rsqrt(jnp.mean(out * out, axis=1, keepdims=True) + EPSILON)
                gate = jax.nn.sigmoid(proj[OUT_GATE, rows, head_cols(h)].astype(F32))
                mix[rows, head_cols(h)] = (out * gain[:, head_cols(h)] * gate).astype(BF16)

    def part_copy(c):
        return pltpu.make_async_remote_copy(
            src_ref=part_send.at[c],
            dst_ref=part_got.at[c],
            send_sem=part_sem_send.at[c],
            recv_sem=part_sem_recv.at[c],
            device_id={"tp": other},
            device_id_type=MESH,
        )

    def partial_rows(index, c):
        return jnp.dot(
            mix[rows_of(index, half), :], out_w[:, rows_of(c, OUT_COLS)], preferred_element_type=F32
        ).astype(BF16)

    readout(other)
    for c in out_copies:
        c.wait()

    @pl.loop(0, n_out)
    def _(c):
        part_send[c] = partial_rows(other, c)
        part_copy(c).start()

    readout(me)

    def result_copy(c):
        return pltpu.make_async_copy(
            result.at[c], layer_out.at[:, rows_of(c, OUT_COLS)], out_sem.at[c]
        )

    @pl.loop(0, n_out)
    def _(c):
        own = partial_rows(me, c)
        part_copy(c).wait_recv()
        result[c] = (own.astype(F32) + part_got[c].astype(F32)).astype(BF16)
        result_copy(c).start()

    token_copy.wait_send()

    @pl.when(place + 1 < n_sp)
    def _():
        rim_copy.wait_send()

    for d in range(1, n_sp):

        @pl.when(place + d < n_sp)
        def _(d=d):
            for c in seg_copies(place + d, place, d - 1):
                c.wait_send()

    @pl.loop(0, n_out)
    def _(c):
        part_copy(c).wait_send()
        result_copy(c).wait()


def local(
    tokens,
    norm_gain,
    w_query,
    w_key,
    w_value,
    w_outgate,
    w_gatein,
    w_gateout,
    w_convin,
    w_igate,
    w_fgate,
    input_bias,
    forget_bias,
    forget_extra,
    init_memory,
    head_gain,
    conv_taps,
    out_memory,
    out_conv,
):
    heads, dh = init_memory.shape[1], init_memory.shape[2]
    half, features = tokens.shape[1], tokens.shape[2]
    rows = forget_extra.shape[1]
    width = w_query.shape[1]
    nblocks = rows // BLOCK
    n_sp = lax.axis_size("sp")
    first = lax.axis_index("tp") * heads

    def own(a, axis):
        return lax.dynamic_slice_in_dim(a, first, heads, axis)

    gate_w = jnp.concatenate(
        [
            own(w_fgate, 1),
            jnp.zeros((features, PAD - heads), BF16),
            own(w_igate, 1),
            jnp.zeros((features, BLOCK - PAD - heads), BF16),
        ],
        axis=1,
    )
    gap = jnp.zeros((PAD - heads,), F32)
    gate_bias = jnp.concatenate([own(forget_bias, 0), gap, own(input_bias, 0), gap])
    gate_bias = jnp.broadcast_to(gate_bias[:, None], (2 * PAD, BLOCK))
    extra = jnp.pad(jnp.transpose(forget_extra[0]), ((0, PAD - heads), (0, 0)))

    vmem = pl.BlockSpec(memory_space=pltpu.VMEM)
    hbm = pl.BlockSpec(memory_space=pl.ANY)
    dma = pltpu.SemaphoreType.DMA
    n_seg = max(n_sp - 1, 1)
    n_out = features // OUT_COLS
    out = pl.pallas_call(
        functools.partial(kernel, n_sp),
        name="layer",
        out_shape=jax.ShapeDtypeStruct((half, features), BF16),
        in_specs=[hbm, vmem] + [hbm] * 7 + [vmem] * 6 + [hbm] * 2,
        out_specs=hbm,
        scratch_shapes=[
            pltpu.VMEM((2, half, features), BF16),
            pltpu.VMEM((rows, features), BF16),
            pltpu.VMEM((7, features, width), BF16),
            pltpu.VMEM((2 * width, features), BF16),
            pltpu.VMEM((7, rows, width), BF16),
            pltpu.VMEM((rows, BLOCK), F32),
            pltpu.VMEM((nblocks, 2 * PAD, BLOCK), F32),
            pltpu.VMEM((nblocks, BLOCK, BLOCK), F32),
            pltpu.VMEM((nblocks, PAD, BLOCK), F32),
            pltpu.VMEM((nblocks, PAD, BLOCK), F32),
            pltpu.VMEM((nblocks, heads, dh, dh), F32),
            pltpu.VMEM((heads, dh, dh), F32),
            pltpu.VMEM((2 * PAD, BLOCK), F32),
            pltpu.VMEM((nblocks, heads, dh, dh), BF16),
            pltpu.VMEM((nblocks, PAD, BLOCK), F32),
            pltpu.VMEM((heads, dh, dh), BF16),
            pltpu.VMEM((2 * PAD, BLOCK), F32),
            pltpu.VMEM((n_seg, heads, dh, dh), BF16),
            pltpu.VMEM((n_seg, 2 * PAD, BLOCK), F32),
            pltpu.VMEM((RIM + rows, width), BF16),
            pltpu.VMEM((RIM, width), BF16),
            pltpu.VMEM((rows, 2 * width), BF16),
            pltpu.VMEM((n_out, half, OUT_COLS), BF16),
            pltpu.VMEM((n_out, half, OUT_COLS), BF16),
            pltpu.VMEM((n_out, half, OUT_COLS), BF16),
            dma((1,)),
            dma((9,)),
            dma((n_out,)),
            dma((2,)),
            dma((2, n_seg)),
            dma((2, n_seg)),
            dma((2,)),
            dma((n_out,)),
            dma((n_out,)),
        ],
        compiler_params=pltpu.CompilerParams(
            collective_id=0, has_side_effects=True, vmem_limit_bytes=63 * 1024 * 1024
        ),
    )(
        tokens[0],
        norm_gain.reshape(1, features),
        w_key,
        w_value,
        w_gatein,
        w_convin,
        w_gateout,
        w_query,
        w_outgate,
        gate_w,
        gate_bias,
        extra,
        init_memory[0],
        head_gain.reshape(1, -1),
        conv_taps,
        out_memory,
        out_conv,
    )
    return out[None]


def solution(mesh):
    return jax.shard_map(
        local,
        mesh=mesh,
        in_specs=(
            P("fs", ("sp", "tp"), None),
            P(),
            P(None, "tp"),
            P(None, "tp"),
            P(None, "tp"),
            P(None, "tp"),
            P(None, "tp"),
            P(None, "tp"),
            P(None, "tp"),
            P(),
            P(),
            P(),
            P(),
            P("fs", "sp", "tp"),
            P("fs", "tp", None, None),
            P(),
            P(),
            P("tp", None),
            P("tp", None),
        ),
        out_specs=P("fs", ("sp", "tp"), None),
        check_vma=False,
    )
```

time: 163 us -> 66.6 us (0.41)
  matrix products: 64.6 us -> 0 us
  Pallas kernels: 0 us -> 53.4 us
  waiting for transfers between devices: 27.7 us -> 0 us
  other arithmetic: 25.9 us -> 1.24 us
  between operations: 14.1 us -> 0.02 us
  blocking collectives: 10.3 us -> 0 us
  local copies, waits for them, and re-layouts: 15 us -> 10.8 us
  starting transfers between devices: 3.92 us -> 0 us
    dot_general x11 -> x0, matrix products: 64.6 us -> none  [the longest x5 23.3 us: project(): jnp.dot(normed_all, weight, preferred_element_type=jnp.float32)]
    pallas_call x0 -> x1, Pallas kernels: none -> 53.4 us  [local(): pl.pallas_call(functools.partial(kernel, n_sp), name='layer', out_shape=j...]
    all_gather x2 -> x0, waiting for transfers between devices: 14.4 us -> none  [the longest x1 14.4 us: local(): normed_all = lax.all_gather(normed, 'tp', axis=0, tiled=True)]
    reduce_scatter x1 -> x0, waiting for transfers between devices: 13.3 us -> none  [local(): lax.psum_scatter((jnp.dot(memory_out, out_memory, preferred_element_type=...]
    unnamed x1 -> x0, blocking collectives: 10.3 us -> none
    add x9 -> x0, other arithmetic: 9.44 us -> none  [compose(): kept_share[..., None, None] * memory]
    reshape x6 -> x2, local copies, waits for them, and re-layouts: 10.4 us -> 2.55 us  [the longest x1 1.28 us: local(): norm_gain.reshape(1, features)]
    dynamic_update_slice x8 -> x0, other arithmetic: 5.83 us -> none  [local(): lax.scan(block_step, identity, (block_total, block_terms, block_top))]
  transfers between devices with their start and end apart: 4 -> 0, of which waited for: 2 -> 0; matrix products, arithmetic and copies ran while one was open for 11% -> 0% of each run, Pallas kernels for 0% -> 0%
where the time goes in v1:
time: 66.6 us; the launch traced here: 65.4 us
  Pallas kernels  53.4 us (80%)
  local copies, waits for them, and re-layouts  10.8 us (16%)
  other arithmetic  1.24 us (2%)
    pallas_call x1, Pallas kernels, local(): pl.pallas_call(functools.partial(kernel, n_sp), name='layer', out_shape=j...  53.4 us
    unnamed x3, local copies, waits for them, and re-layouts  3.79 us
    dynamic_slice x3, local copies, waits for them, and re-layouts, own(): return lax.dynamic_slice_in_dim(a, first, heads, axis)  2.25 us
    pad x1, local copies, waits for them, and re-layouts, local(): extra = jnp.pad(jnp.transpose(forget_extra[0]), ((0, PAD - heads), (0, 0)))  1.34 us

profile of v1, /device:TPU:0, one launch (start us, length us, event | category | flops | bytes accessed | tf_op | source)
XLA Modules:
  0.0 65.4 jit_solution(10527737679192170173)
XLA Ops:
  0.0 0.7 %dynamic_slice.15 = f32[4]{0:T(128)S(1)} dynamic-slice(f32[8]{0:T(128)} %param.30, s32[]{:T(128)S(6)} %select_n.2), dynamic_slice_sizes={4} | dynamic-slice | bytes 36 | tf_op jit(solution)/shard_map/dynamic_slice | solution.py:444
  0.7 0.7 %dynamic_slice.14 = f32[4]{0:T(128)S(1)} dynamic-slice(f32[8]{0:T(128)} %param.31, s32[]{:T(128)S(6)} %select_n.2), dynamic_slice_sizes={4} | dynamic-slice | bytes 36 | tf_op jit(solution)/shard_map/dynamic_slice | solution.py:444
  1.5 0.1 pad.12.clone
  1.5 0.1 pad.10.clone
  1.6 0.1 pad_maximum_fusion
  1.7 1.3 %reshape.8.head_gain = bf16[1,1024]{1,0:T(2,128)(2,1)} reshape(bf16[1024]{0:T(1024)(128)(2,1)} %param.34) | data formatting | bytes 4096 | tf_op jit(solution)/shard_map/reshape | solution.py:524
  3.0 0.7 %broadcast_in_dim.17.gate_bias = f32[16,128]{1,0:T(8,128)} broadcast(f32[16]{0:T(128)S(1)} %pad_maximum_fusion), dimensions={0} | broadcast | bytes 8256 | tf_op jit(solution)/shard_map/broadcast_in_dim | solution.py:457
  3.6 1.3 %reshape.7.norm_gain = bf16[1,2048]{1,0:T(2,128)(2,1)} reshape(bf16[2048]{0:T(1024)(128)(2,1)} %param.20) | data formatting | bytes 8192 | tf_op jit(solution)/shard_map/reshape | solution.py:512
  4.9 0.8 %constant_dynamic-slice_fusion = (bf16[2048,4]{0,1:T(4,128)(2,1)S(1)}, bf16[2048,4]{0,1:T(4,128)(2,1)S(1)}) fusion(bf16[2048,8]{0,1:T(8,128)(2,1)} %param.28, s32[]{:T(128)S(6)} %select_n.2, bf16[2048,8]{0,1:T(8,128)(2,1)} %param.29), kind=kLoop, calls=%fused_computation.2 | loop fusion | bytes 65540 | tf_op jit(solution)/shard_map/dynamic_slice | solution.py:444
  5.7 1.3 %pad.4.extra = f32[8,1024]{1,0:T(8,128)} pad(f32[4,1024]{1,0:T(4,128)} %bitcast.9, f32[]{:T(128)} %constant.5.clone.1), padding=0_4x0_0 | pad | bytes 49156 | tf_op jit(solution)/shard_map/jit(_pad)/pad | solution.py:458
  7.1 0.3 copy.23
  7.4 0.3 copy.22
  7.7 1.2 %maximum_maximum_fusion.gate_w = bf16[2048,128]{1,0:T(8,128)(2,1)} fusion(bf16[2048,4]{1,0:T(8,128)(2,1)S(1)} %copy.23, bf16[2048,4]{1,0:T(8,128)(2,1)S(1)} %copy.22, bf16[128]{0:T(256)(128)(2,1)S(1)} %pad.12.clone, bf16[128]{0:T(256)(128)(2,1)S(1)} %pad.10.clone), kind=kLoop, calls=%fused_computation | loop fusion | flops 2097152 | bytes 557568 | tf_op jit(solution)/shard_map/concatenate | solution.py:446
  8.9 53.4 %layer.1 = bf16[512,2048]{1,0:T(8,128)(2,1)} custom-call(bf16[512,2048]{1,0:T(8,128)(2,1)} %bitcast.7, bf16[1,2048]{1,0:T(2,128)(2,1)} %reshape.7.norm_gain, bf16[2048,512]{1,0:T(8,128)(2,1)} %w_key.1, bf16[2048,512]{1,0:T(8,128)(2,1)} %w_value.1, bf16[2048,512]{1,0:T(8,128)(2,1)} %w_gatein.1, bf16[2048,512]{1,0:T(8,128)(2,1)} %w_convin.1, ...), custom_call_target="tpu_custom_call" | custom-call | tf_op jit(solution)/shard_map/layer/pallas_call | solution.py:465
  62.3 3.2 %copy.25 = bf16[1,512,2048]{2,1,0:T(8,128)(2,1)} copy(bf16[1,512,2048]{2,1,0:T(8,128)(2,1)} %bitcast.6) | data formatting | bytes 4194304
  (3 shorter events, 0.0 us)

commit v2 on v1

--- a/solution.py
+++ b/solution.py
@@ -16,7 +16,6 @@
 PAD = 8
 RIM = 16
 NORM_ROWS = 64
-OUT_COLS = 512
 
 KEY, VALUE, GATE_IN, CONV_IN, GATE_OUT, QUERY, OUT_GATE = range(7)
 
@@ -32,8 +31,10 @@
     w_gateout,
     w_query,
     w_outgate,
-    gate_w,
-    gate_bias,
+    w_igate,
+    w_fgate,
+    input_bias,
+    forget_bias,
     extra,
     init_memory,
     head_gain,
@@ -42,6 +43,9 @@
     out_conv,
     layer_out,
     tok,
+    gain_row,
+    head_rows,
+    gate_w,
     normed,
     weights,
     out_w,
@@ -65,10 +69,8 @@
     mix,
     part_send,
     part_got,
-    result,
     local_sem,
     weight_sem,
-    out_sem,
     token_sem,
     seg_send,
     seg_recv,
@@ -87,7 +89,8 @@
     nblocks = total_rows // BLOCK
     key_factor = dh ** (-0.5)
     out_width = layer_out.shape[1]
-    n_out = out_width // OUT_COLS
+    n_out = half // BLOCK
+    out_cols = out_width // n_out
 
     barrier = pltpu.get_barrier_semaphore()
     pl.semaphore_signal(barrier, inc=1, device_id={"tp": other}, device_id_type=MESH)
@@ -119,6 +122,14 @@
         device_id_type=MESH,
     )
     token_copy.start()
+
+    gates = jnp.concatenate(
+        [w_fgate[...], w_igate[...], jnp.zeros((BLOCK - 2 * PAD, w_igate.shape[1]), BF16)], axis=0
+    )
+    gate_w[...] = jnp.transpose(gates)
+    for j in range(norm_gain.shape[0]):
+        gain_row[:, j * BLOCK : (j + 1) * BLOCK] = norm_gain[j : j + 1].astype(F32)
+    head_rows[...] = head_gain[...].astype(F32)
     own_copy.wait()
 
     def rows_of(index, size):
@@ -129,7 +140,7 @@
         def _(c):
             x = tok[slot, rows_of(c, NORM_ROWS), :].astype(F32)
             scale = lax.rsqrt(jnp.mean(x * x, axis=-1, keepdims=True) + EPSILON)
-            y = (x * scale) * norm_gain[...].astype(F32)
+            y = (x * scale) * gain_row[...]
             normed[pl.ds(pl.multiple_of(base + c * NORM_ROWS, NORM_ROWS), NORM_ROWS), :] = y.astype(
                 BF16
             )
@@ -170,31 +181,51 @@
     def head_cols(h):
         return slice(h * dh, (h + 1) * dh)
 
-    @pl.loop(0, nblocks)
+    first_head = me * heads
+    to_front = lax.rem(PAD - first_head, PAD)
+    lane_head = lax.broadcasted_iota(jnp.int32, (PAD, BLOCK), 0)
+    bias_f = jnp.zeros((PAD, BLOCK), F32)
+    bias_i = jnp.zeros((PAD, BLOCK), F32)
+    for h in range(heads):
+        bias_f = jnp.where(lane_head == h, forget_bias[first_head + h], bias_f)
+        bias_i = jnp.where(lane_head == h, input_bias[first_head + h], bias_i)
+    no_head = jnp.zeros((PAD - heads, BLOCK), F32)
+
+    forget_rows, in_rows = [], []
+    for b in range(nblocks):
+        span = slice(b * BLOCK, (b + 1) * BLOCK)
+        pre = jnp.transpose(gate_pre[span, :])
+        v = pltpu.roll(pre[0:PAD], to_front, 0) + bias_f
+        log_forget = jnp.minimum(v, 0.0) - jnp.log1p(jnp.exp(-jnp.abs(v)))
+        forget_rows.append(log_forget + jnp.concatenate([extra[:, span], no_head], axis=0))
+        in_rows.append(pltpu.roll(pre[PAD : 2 * PAD], to_front, 0) + bias_i)
+    all_cumulative = jnp.dot(
+        jnp.concatenate(forget_rows, axis=0),
+        upper,
+        precision=lax.Precision.HIGHEST,
+        preferred_element_type=F32,
+    )
+    all_in = jnp.concatenate(in_rows, axis=0)
+    all_total = jnp.broadcast_to(all_cumulative[:, BLOCK - 1 : BLOCK], all_in.shape)
+    exponent = all_total - all_cumulative + all_in
+    all_peak = jnp.broadcast_to(jnp.max(exponent, axis=1, keepdims=True), all_in.shape)
+    key_weight = jnp.exp(exponent - all_peak)
+    filler = jnp.zeros((BLOCK - 2 * PAD, BLOCK), F32)
+    for b in range(nblocks):
+        span = slice(b * PAD, (b + 1) * PAD)
+        row_log[b, 0:PAD] = all_cumulative[span]
+        row_log[b, PAD : 2 * PAD] = all_in[span]
+        block_sum[b] = all_total[span]
+        block_peak[b] = all_peak[span]
+        col_log[b] = jnp.transpose(
+            jnp.concatenate([all_cumulative[span], key_weight[span], filler], axis=0)
+        )
+
+    @pl.loop(0, nblocks, unroll=2)
     def _(b):
         rows = rows_of(b, BLOCK)
-        pre = jnp.transpose(gate_pre[rows, :])
-        v = pre[0:PAD] + gate_bias[0:PAD]
-        log_forget = jnp.minimum(v, 0.0) - jnp.log1p(jnp.exp(-jnp.abs(v))) + extra[:, rows]
-        gate_in = pre[PAD : 2 * PAD] + gate_bias[PAD : 2 * PAD]
-        cumulative = jnp.dot(
-            log_forget, upper, precision=lax.Precision.HIGHEST, preferred_element_type=F32
-        )
-        total = cumulative[:, BLOCK - 1 : BLOCK]
-        exponent = total - cumulative + gate_in
-        peak = jnp.max(exponent, axis=1, keepdims=True)
-        key_weight = jnp.exp(exponent - peak)
-        row_log[b, 0:PAD] = cumulative
-        row_log[b, PAD : 2 * PAD] = gate_in
-        stacked = jnp.concatenate(
-            [cumulative, key_weight, jnp.zeros((BLOCK - 2 * PAD, BLOCK), F32)], axis=0
-        )
-        columns = jnp.transpose(stacked)
-        col_log[b] = columns
-        total = jnp.broadcast_to(total, (PAD, BLOCK))
-        peak = jnp.broadcast_to(peak, (PAD, BLOCK))
-        block_sum[b] = total
-        block_peak[b] = peak
+        columns = col_log[b]
+        total, peak = block_sum[b], block_peak[b]
         old_log = running_log[0:PAD]
         merged = jnp.maximum(total + old_log, peak)
         keep = jnp.exp(total + old_log - merged)
@@ -325,34 +356,30 @@
             starts[b, h] = running[h].astype(BF16)
         advance(block_sum[b], block_peak[b], lambda h: terms[b, h])
 
-    gain = head_gain[:, own_cols].astype(F32)
     causal = col_i <= row_i
 
-    def readout(index):
-        @pl.loop(0, half // BLOCK)
-        def _(step):
-            b = index * (half // BLOCK) + step
-            rows = rows_of(b, BLOCK)
-            columns = col_log[b]
-            for h in range(heads):
-                q = proj[QUERY, rows, head_cols(h)]
-                k = proj[KEY, rows, head_cols(h)]
-                scores = lax.dot_general(
-                    q, k, (((1,), (1,)), ((), ())), preferred_element_type=F32
-                )
-                cum_col = columns[:, h : h + 1]
-                pair = (cum_col - row_log[b, h : h + 1]) + row_log[b, PAD + h : PAD + h + 1]
-                pair = jnp.where(causal, pair, -jnp.inf)
-                carried_log = cum_col + starts_log[b, h : h + 1, 0:1]
-                top = jnp.maximum(carried_log, jnp.max(pair, axis=1, keepdims=True))
-                weighted = (jnp.exp(pair - top) * (scores * key_factor)).astype(BF16)
-                carried = jnp.dot(q, starts[b, h], preferred_element_type=F32)
-                out = jnp.exp(carried_log - top) * carried + jnp.dot(
-                    weighted, proj[VALUE, rows, head_cols(h)], preferred_element_type=F32
-                )
-                out = out * lax.rsqrt(jnp.mean(out * out, axis=1, keepdims=True) + EPSILON)
-                gate = jax.nn.sigmoid(proj[OUT_GATE, rows, head_cols(h)].astype(F32))
-                mix[rows, head_cols(h)] = (out * gain[:, head_cols(h)] * gate).astype(BF16)
+    def read_block(b):
+        rows = rows_of(b, BLOCK)
+        columns = col_log[b]
+        for h in range(heads):
+            q = proj[QUERY, rows, head_cols(h)]
+            k = proj[KEY, rows, head_cols(h)]
+            scores = lax.dot_general(
+                q, k, (((1,), (1,)), ((), ())), preferred_element_type=F32
+            )
+            cum_col = columns[:, h : h + 1]
+            pair = (cum_col - row_log[b, h : h + 1]) + row_log[b, PAD + h : PAD + h + 1]
+            pair = jnp.where(causal, pair, -jnp.inf)
+            carried_log = cum_col + starts_log[b, h : h + 1, 0:1]
+            top = jnp.maximum(carried_log, jnp.max(pair, axis=1, keepdims=True))
+            weighted = (jnp.exp(pair - top) * (scores * key_factor)).astype(BF16)
+            carried = jnp.dot(q, starts[b, h], preferred_element_type=F32)
+            out = jnp.exp(carried_log - top) * carried + jnp.dot(
+                weighted, proj[VALUE, rows, head_cols(h)], preferred_element_type=F32
+            )
+            out = out * lax.rsqrt(jnp.mean(out * out, axis=1, keepdims=True) + EPSILON)
+            gate = jax.nn.sigmoid(proj[OUT_GATE, rows, head_cols(h)].astype(F32))
+            mix[rows, head_cols(h)] = (out * head_rows[pl.ds(first_head + h, 1), :] * gate).astype(BF16)
 
     def part_copy(c):
         return pltpu.make_async_remote_copy(
@@ -366,31 +393,28 @@
 
     def partial_rows(index, c):
         return jnp.dot(
-            mix[rows_of(index, half), :], out_w[:, rows_of(c, OUT_COLS)], preferred_element_type=F32
+            mix[rows_of(index, half), :], out_w[:, rows_of(c, out_cols)], preferred_element_type=F32
         ).astype(BF16)
 
-    readout(other)
+    @pl.loop(0, n_out)
+    def _(step):
+        read_block(other * n_out + step)
+
     for c in out_copies:
         c.wait()
 
     @pl.loop(0, n_out)
-    def _(c):
-        part_send[c] = partial_rows(other, c)
-        part_copy(c).start()
-
-    readout(me)
-
-    def result_copy(c):
-        return pltpu.make_async_copy(
-            result.at[c], layer_out.at[:, rows_of(c, OUT_COLS)], out_sem.at[c]
-        )
+    def _(step):
+        part_send[step] = partial_rows(other, step)
+        read_block(me * n_out + step)
+        part_copy(step).start()
 
     @pl.loop(0, n_out)
     def _(c):
         own = partial_rows(me, c)
         part_copy(c).wait_recv()
-        result[c] = (own.astype(F32) + part_got[c].astype(F32)).astype(BF16)
-        result_copy(c).start()
+        total = own.astype(F32) + part_got[c].astype(F32)
+        layer_out[:, rows_of(c, out_cols)] = total.astype(BF16)
 
     token_copy.wait_send()
 
@@ -408,7 +432,6 @@
     @pl.loop(0, n_out)
     def _(c):
         part_copy(c).wait_send()
-        result_copy(c).wait()
 
 
 def local(
@@ -438,38 +461,24 @@
     width = w_query.shape[1]
     nblocks = rows // BLOCK
     n_sp = lax.axis_size("sp")
-    first = lax.axis_index("tp") * heads
-
-    def own(a, axis):
-        return lax.dynamic_slice_in_dim(a, first, heads, axis)
-
-    gate_w = jnp.concatenate(
-        [
-            own(w_fgate, 1),
-            jnp.zeros((features, PAD - heads), BF16),
-            own(w_igate, 1),
-            jnp.zeros((features, BLOCK - PAD - heads), BF16),
-        ],
-        axis=1,
-    )
-    gap = jnp.zeros((PAD - heads,), F32)
-    gate_bias = jnp.concatenate([own(forget_bias, 0), gap, own(input_bias, 0), gap])
-    gate_bias = jnp.broadcast_to(gate_bias[:, None], (2 * PAD, BLOCK))
-    extra = jnp.pad(jnp.transpose(forget_extra[0]), ((0, PAD - heads), (0, 0)))
-
     vmem = pl.BlockSpec(memory_space=pltpu.VMEM)
     hbm = pl.BlockSpec(memory_space=pl.ANY)
+    smem = pl.BlockSpec(memory_space=pltpu.SMEM)
     dma = pltpu.SemaphoreType.DMA
     n_seg = max(n_sp - 1, 1)
-    n_out = features // OUT_COLS
+    n_out = half // BLOCK
+    out_cols = features // n_out
     out = pl.pallas_call(
         functools.partial(kernel, n_sp),
         name="layer",
-        out_shape=jax.ShapeDtypeStruct((half, features), BF16),
-        in_specs=[hbm, vmem] + [hbm] * 7 + [vmem] * 6 + [hbm] * 2,
-        out_specs=hbm,
+        out_shape=pltpu.VMEM((half, features), BF16),
+        in_specs=[hbm, vmem] + [hbm] * 7 + [vmem] * 2 + [smem] * 2 + [vmem] * 4 + [hbm] * 2,
+        out_specs=vmem,
         scratch_shapes=[
             pltpu.VMEM((2, half, features), BF16),
+            pltpu.VMEM((1, features), F32),
+            pltpu.VMEM((PAD, BLOCK), F32),
+            pltpu.VMEM((features, BLOCK), BF16),
             pltpu.VMEM((rows, features), BF16),
             pltpu.VMEM((7, features, width), BF16),
             pltpu.VMEM((2 * width, features), BF16),
@@ -491,12 +500,10 @@
             pltpu.VMEM((RIM + rows, width), BF16),
             pltpu.VMEM((RIM, width), BF16),
             pltpu.VMEM((rows, 2 * width), BF16),
-            pltpu.VMEM((n_out, half, OUT_COLS), BF16),
-            pltpu.VMEM((n_out, half, OUT_COLS), BF16),
-            pltpu.VMEM((n_out, half, OUT_COLS), BF16),
+            pltpu.VMEM((n_out, half, out_cols), BF16),
+            pltpu.VMEM((n_out, half, out_cols), BF16),
             dma((1,)),
             dma((9,)),
-            dma((n_out,)),
             dma((2,)),
             dma((2, n_seg)),
             dma((2, n_seg)),
@@ -505,11 +512,11 @@
             dma((n_out,)),
         ],
         compiler_params=pltpu.CompilerParams(
-            collective_id=0, has_side_effects=True, vmem_limit_bytes=63 * 1024 * 1024
+            collective_id=0, has_side_effects=True, vmem_limit_bytes=60 * 1024 * 1024
         ),
     )(
         tokens[0],
-        norm_gain.reshape(1, features),
+        norm_gain.reshape(-1, BLOCK),
         w_key,
         w_value,
         w_gatein,
@@ -517,11 +524,13 @@
         w_gateout,
         w_query,
         w_outgate,
-        gate_w,
-        gate_bias,
-        extra,
+        jnp.transpose(w_igate),
+        jnp.transpose(w_fgate),
+        input_bias,
+        forget_bias,
+        jnp.transpose(forget_extra[0]),
         init_memory[0],
-        head_gain.reshape(1, -1),
+        head_gain.reshape(-1, dh),
         conv_taps,
         out_memory,
         out_conv,

time: 66.6 us -> 48.4 us (0.73)
  local copies, waits for them, and re-layouts: 10.8 us -> 1.32 us
  Pallas kernels: 53.4 us -> 46.2 us
  other arithmetic: 1.24 us -> 0 us
    pallas_call x1, Pallas kernels: 53.4 us -> 46.2 us  [local(): pl.pallas_call(functools.partial(kernel, n_sp), name='layer', out_shape=p...]
    reshape x2 -> x0, local copies, waits for them, and re-layouts: 2.55 us -> none  [the longest x1 1.28 us: local(): norm_gain.reshape(1, features)]
    unnamed x3 -> x1, local copies, waits for them, and re-layouts: 3.79 us -> 1.32 us
    dynamic_slice x3 -> x0, local copies, waits for them, and re-layouts: 2.25 us -> none  [own(): return lax.dynamic_slice_in_dim(a, first, heads, axis)]
    pad x1 -> x0, local copies, waits for them, and re-layouts: 1.34 us -> none  [local(): extra = jnp.pad(jnp.transpose(forget_extra[0]), ((0, PAD - heads), (0, 0)))]
    concatenate x2 -> x0, other arithmetic: 1.24 us -> none  [the longest x1 1.16 us: local(): jnp.concatenate([own(w_fgate, 1), jnp.zeros((features, PAD - heads), BF16...]
    broadcast_in_dim x3 -> x0, local copies, waits for them, and re-layouts: 0.67 us -> none  [the longest x1 0.67 us: local(): gate_bias = jnp.broadcast_to(gate_bias[:, None], (2 * PAD, BLOCK))]
where the time goes in v2:
time: 48.4 us; the launch traced here: 47.5 us
  Pallas kernels  46.2 us (95%)
  local copies, waits for them, and re-layouts  1.32 us (3%)
    pallas_call x1, Pallas kernels, local(): pl.pallas_call(functools.partial(kernel, n_sp), name='layer', out_shape=p...  46.2 us
    unnamed x1, local copies, waits for them, and re-layouts  1.32 us

profile of v2, /device:TPU:0, one launch (start us, length us, event | category | flops | bytes accessed | tf_op | source)
XLA Modules:
  0.0 47.5 jit_solution(14435158206336123296)
XLA Ops:
  0.0 46.2 %layer.1 = bf16[512,2048]{1,0:T(8,128)(2,1)S(1)} custom-call(bf16[512,2048]{1,0:T(8,128)(2,1)} %bitcast.11, bf16[16,128]{1,0:T(8,128)(2,1)} %bitcast.16, bf16[2048,512]{1,0:T(8,128)(2,1)} %w_key.1, bf16[2048,512]{1,0:T(8,128)(2,1)} %w_value.1, bf16[2048,512]{1,0:T(8,128)(2,1)} %w_gatein.1, bf16[2048,512]{1,0:T(8,128)(2,1)} %w_convin.1, ...), custom_call_target="tpu_custom_call" | custom-call | tf_op jit(solution)/shard_map/layer/pallas_call | solution.py:471
  46.2 1.3 %copy.21 = bf16[1,512,2048]{2,1,0:T(8,128)(2,1)} copy(bf16[1,512,2048]{2,1,0:T(8,128)(2,1)S(1)} %bitcast.10) | data formatting | bytes 4194304

commit v3 on v2

--- a/solution.py
+++ b/solution.py
@@ -17,7 +17,7 @@
 RIM = 16
 NORM_ROWS = 64
 
-KEY, VALUE, GATE_IN, CONV_IN, GATE_OUT, QUERY, OUT_GATE = range(7)
+KEY, VALUE, QUERY, GATE_IN, CONV_IN, GATE_OUT, OUT_GATE = range(7)
 
 
 def kernel(
@@ -56,6 +56,8 @@
     block_sum,
     block_peak,
     terms,
+    within,
+    peak_log,
     running,
     running_log,
     starts,
@@ -101,7 +103,7 @@
 
     own_copy = pltpu.make_async_copy(tokens, tok.at[0], local_sem.at[0])
     own_copy.start()
-    w_in = (w_key, w_value, w_gatein, w_convin, w_gateout, w_query, w_outgate)
+    w_in = (w_key, w_value, w_query, w_gatein, w_convin, w_gateout, w_outgate)
     w_copies = [
         pltpu.make_async_copy(w, weights.at[s], weight_sem.at[s]) for s, w in enumerate(w_in)
     ]
@@ -109,7 +111,7 @@
         pltpu.make_async_copy(out_memory, out_w.at[pl.ds(0, width)], weight_sem.at[7]),
         pltpu.make_async_copy(out_conv, out_w.at[pl.ds(width, width)], weight_sem.at[8]),
     ]
-    for c in w_copies + out_copies:
+    for c in w_copies[:2]:
         c.start()
 
     pl.semaphore_wait(barrier, n_sp)
@@ -131,6 +133,8 @@
         gain_row[:, j * BLOCK : (j + 1) * BLOCK] = norm_gain[j : j + 1].astype(F32)
     head_rows[...] = head_gain[...].astype(F32)
     own_copy.wait()
+    for c in w_copies[2:] + out_copies:
+        c.start()
 
     def rows_of(index, size):
         return pl.ds(pl.multiple_of(index * size, size), size)
@@ -268,14 +272,50 @@
             for c in seg_copies(place + d, place, d - 1):
                 c.start()
 
+    causal = col_i <= row_i
+
+    def own_terms(b):
+        rows = rows_of(b, BLOCK)
+        columns = col_log[b]
+        for h in range(heads):
+            q = proj[QUERY, rows, head_cols(h)]
+            k = proj[KEY, rows, head_cols(h)]
+            scores = lax.dot_general(q, k, (((1,), (1,)), ((), ())), preferred_element_type=F32)
+            pair = (columns[:, h : h + 1] - row_log[b, h : h + 1]) + row_log[
+                b, PAD + h : PAD + h + 1
+            ]
+            pair = jnp.where(causal, pair, -jnp.inf)
+            peak = jnp.max(pair, axis=1, keepdims=True)
+            weighted = (jnp.exp(pair - peak) * (scores * key_factor)).astype(BF16)
+            peak_log[b, :, h : h + 1] = peak
+            within[b, h] = jnp.dot(
+                weighted, proj[VALUE, rows, head_cols(h)], preferred_element_type=F32
+            )
+
+    def weight_wait(slot):
+        pltpu.make_async_copy(w_key, weights.at[slot], weight_sem.at[slot]).wait()
+
+    weight_wait(QUERY)
+
+    @pl.loop(0, 2)
+    def _(index):
+        project(QUERY, rows_of(index, half))
+
+    per_job = nblocks // 8
+
     def finish(slots):
-        @pl.loop(slots[0], slots[1])
-        def _(slot):
-            pltpu.make_async_copy(w_key, weights.at[slot], weight_sem.at[slot]).wait()
-
-            @pl.loop(0, 2)
-            def _(index):
-                project(slot, rows_of(index, half))
+        @pl.loop(2 * slots[0], 2 * slots[1])
+        def _(job):
+            slot = job // 2
+            index = lax.rem(job, 2)
+
+            @pl.when(index == 0)
+            def _():
+                weight_wait(slot)
+
+            project(slot, rows_of(index, half))
+            for i in range(per_job):
+                own_terms((job - 2 * GATE_IN) * per_job + i)
 
     finish((GATE_IN, CONV_IN + 1))
 
@@ -356,30 +396,21 @@
             starts[b, h] = running[h].astype(BF16)
         advance(block_sum[b], block_peak[b], lambda h: terms[b, h])
 
-    causal = col_i <= row_i
-
     def read_block(b):
         rows = rows_of(b, BLOCK)
         columns = col_log[b]
         for h in range(heads):
-            q = proj[QUERY, rows, head_cols(h)]
-            k = proj[KEY, rows, head_cols(h)]
-            scores = lax.dot_general(
-                q, k, (((1,), (1,)), ((), ())), preferred_element_type=F32
+            peak = peak_log[b, :, h : h + 1]
+            carried_log = columns[:, h : h + 1] + starts_log[b, h : h + 1, 0:1]
+            top = jnp.maximum(carried_log, peak)
+            carried = jnp.dot(
+                proj[QUERY, rows, head_cols(h)], starts[b, h], preferred_element_type=F32
             )
-            cum_col = columns[:, h : h + 1]
-            pair = (cum_col - row_log[b, h : h + 1]) + row_log[b, PAD + h : PAD + h + 1]
-            pair = jnp.where(causal, pair, -jnp.inf)
-            carried_log = cum_col + starts_log[b, h : h + 1, 0:1]
-            top = jnp.maximum(carried_log, jnp.max(pair, axis=1, keepdims=True))
-            weighted = (jnp.exp(pair - top) * (scores * key_factor)).astype(BF16)
-            carried = jnp.dot(q, starts[b, h], preferred_element_type=F32)
-            out = jnp.exp(carried_log - top) * carried + jnp.dot(
-                weighted, proj[VALUE, rows, head_cols(h)], preferred_element_type=F32
-            )
+            out = jnp.exp(carried_log - top) * carried + jnp.exp(peak - top) * within[b, h]
             out = out * lax.rsqrt(jnp.mean(out * out, axis=1, keepdims=True) + EPSILON)
             gate = jax.nn.sigmoid(proj[OUT_GATE, rows, head_cols(h)].astype(F32))
-            mix[rows, head_cols(h)] = (out * head_rows[pl.ds(first_head + h, 1), :] * gate).astype(BF16)
+            head = head_rows[pl.ds(first_head + h, 1), :]
+            mix[rows, head_cols(h)] = (out * head * gate).astype(BF16)
 
     def part_copy(c):
         return pltpu.make_async_remote_copy(
@@ -489,6 +520,8 @@
             pltpu.VMEM((nblocks, PAD, BLOCK), F32),
             pltpu.VMEM((nblocks, PAD, BLOCK), F32),
             pltpu.VMEM((nblocks, heads, dh, dh), F32),
+            pltpu.VMEM((nblocks, heads, BLOCK, dh), F32),
+            pltpu.VMEM((nblocks, BLOCK, BLOCK), F32),
             pltpu.VMEM((heads, dh, dh), F32),
             pltpu.VMEM((2 * PAD, BLOCK), F32),
             pltpu.VMEM((nblocks, heads, dh, dh), BF16),

time: 48.4 us -> 49 us (1.012); the launches traced: 47.5 us -> 48.8 us
  Pallas kernels: 46.2 us -> 47.5 us
    pallas_call x1, Pallas kernels: 46.2 us -> 47.5 us  [local(): pl.pallas_call(functools.partial(kernel, n_sp), name='layer', out_shape=p...]
where the time goes in v3:
time: 49 us; the launch traced here: 48.8 us
  Pallas kernels  47.5 us (97%)
  local copies, waits for them, and re-layouts  1.32 us (3%)
    pallas_call x1, Pallas kernels, local(): pl.pallas_call(functools.partial(kernel, n_sp), name='layer', out_shape=p...  47.5 us
    unnamed x1, local copies, waits for them, and re-layouts  1.32 us

profile of v3, /device:TPU:0, one launch (start us, length us, event | category | flops | bytes accessed | tf_op | source)
XLA Modules:
  0.0 48.8 jit_solution(9649251374675852325)
XLA Ops:
  0.0 47.5 %layer.1 = bf16[512,2048]{1,0:T(8,128)(2,1)S(1)} custom-call(bf16[512,2048]{1,0:T(8,128)(2,1)} %bitcast.11, bf16[16,128]{1,0:T(8,128)(2,1)} %bitcast.16, bf16[2048,512]{1,0:T(8,128)(2,1)} %w_key.1, bf16[2048,512]{1,0:T(8,128)(2,1)} %w_value.1, bf16[2048,512]{1,0:T(8,128)(2,1)} %w_gatein.1, bf16[2048,512]{1,0:T(8,128)(2,1)} %w_convin.1, ...), custom_call_target="tpu_custom_call" | custom-call | tf_op jit(solution)/shard_map/layer/pallas_call | solution.py:502
  47.5 1.3 %copy.21 = bf16[1,512,2048]{2,1,0:T(8,128)(2,1)} copy(bf16[1,512,2048]{2,1,0:T(8,128)(2,1)S(1)} %bitcast.10) | data formatting | bytes 4194304

commit v4 on v3

--- a/solution.py
+++ b/solution.py
@@ -313,9 +313,9 @@
             def _():
                 weight_wait(slot)
 
-            project(slot, rows_of(index, half))
             for i in range(per_job):
                 own_terms((job - 2 * GATE_IN) * per_job + i)
+            project(slot, rows_of(index, half))
 
     finish((GATE_IN, CONV_IN + 1))
 

time: 49 us -> 49.1 us (level)
  no operation moved by 1% of the time
where the time goes in v4:
time: 49.1 us; the launch traced here: 49 us
  Pallas kernels  47.6 us (97%)
  local copies, waits for them, and re-layouts  1.32 us (3%)
    pallas_call x1, Pallas kernels, local(): pl.pallas_call(functools.partial(kernel, n_sp), name='layer', out_shape=p...  47.6 us
    unnamed x1, local copies, waits for them, and re-layouts  1.32 us

profile of v4, /device:TPU:0, one launch (start us, length us, event | category | flops | bytes accessed | tf_op | source)
XLA Modules:
  0.0 49.0 jit_solution(10625131909326062088)
XLA Ops:
  0.0 47.6 %layer.1 = bf16[512,2048]{1,0:T(8,128)(2,1)S(1)} custom-call(bf16[512,2048]{1,0:T(8,128)(2,1)} %bitcast.11, bf16[16,128]{1,0:T(8,128)(2,1)} %bitcast.16, bf16[2048,512]{1,0:T(8,128)(2,1)} %w_key.1, bf16[2048,512]{1,0:T(8,128)(2,1)} %w_value.1, bf16[2048,512]{1,0:T(8,128)(2,1)} %w_gatein.1, bf16[2048,512]{1,0:T(8,128)(2,1)} %w_convin.1, ...), custom_call_target="tpu_custom_call" | custom-call | tf_op jit(solution)/shard_map/layer/pallas_call | solution.py:502
  47.7 1.3 %copy.21 = bf16[1,512,2048]{2,1,0:T(8,128)(2,1)} copy(bf16[1,512,2048]{2,1,0:T(8,128)(2,1)S(1)} %bitcast.10) | data formatting | bytes 4194304
